TPU v7x, 32 devices: a whole 2x2x4 slice. The times are simulated.
32 devices in a mesh: sp: 4 (over y, x), tp: 8 (over z, core).
Axes of the slice: x: 2, y: 2, z: 4, core: 2. Of those that a mesh axis runs over, the one named last changes fastest.
Arguments:
- query_a: bfloat16 [512, 16, 256], P('sp', 'tp'), may hold values from -5.5 to 5.5
- key_a: bfloat16 [512, 16, 256], P('sp', 'tp'), may hold values from -5.5 to 5.5
- value_a: bfloat16 [512, 16, 256], P('sp', 'tp'), may hold values from -6 to 6
- query_b: bfloat16 [512, 16, 128], P('sp', 'tp'), may hold values from -5.5 to 5.5
- key_b: bfloat16 [512, 16, 128], P('sp', 'tp'), may hold values from -5.5 to 5.5
- value_b: bfloat16 [512, 16, 128], P('sp', 'tp'), may hold values from -6 to 6
- lambdas: float32 [2, 16], P(None, 'tp'), may hold values from 0.3 to 0.8
- gain_a: float32 [256], replicated, may hold values from 0.1 to 1.9
- gain_b: float32 [128], replicated, may hold values from 0.1 to 1.9
- out_a: bfloat16 [4096, 4096], P('tp'), may hold values from -0.078125 to 0.078125
- out_b: bfloat16 [2048, 4096], P('tp'), may hold values from -0.078125 to 0.078125
- residual: bfloat16 [512, 4096], P(('sp', 'tp')), may hold values from -6 to 6
- norm_gain: float32 [4096], replicated, may hold values from 0.1 to 1.9
- route_ids: int32 [512, 2], P(('sp', 'tp')), may hold values from 0 to 7, all different within a row; in each aligned block of 16 rows (0 to 15, 16 to 31, ...) at most 8 rows name the same one
- route_weights: float32 [512, 2], P(('sp', 'tp')), may hold values from 0.1 to 0.9
- w_gate: bfloat16 [8, 4096, 2048], P('sp', None, 'tp'), may hold values from -0.28125 to 0.28125
- w_up: bfloat16 [8, 4096, 2048], P('sp', None, 'tp'), may hold values from -0.28125 to 0.28125
- w_down: bfloat16 [8, 2048, 4096], P('sp', 'tp'), may hold values from -0.01977539 to 0.01977539
Outputs:
- result: bfloat16 [512, 4096], P(('sp', 'tp'))
Inputs may be any that keep to these rules, and one draw needn't show every extreme that they name: `route_ids`: in the rows of one device each token names 2 different experts, no expert is named more than 8 times, a bound that some block reaches.
All inputs are finite; a program needn't handle non-finite values.
Results may differ from a plain program's by a relative error of at most 0.02.
Values may be sent and summed in bfloat16 or wider, within the bound.
A program may use at most 128 MiB of HBM per device.

v0:
```python
import jax
import jax.numpy as jnp
from jax import lax
from jax.sharding import PartitionSpec as P

EPSILON = 1e-06
LIMIT = 7.0
SLOPE = 1.702
FLOOR = -1e30


def empty_state(heads_here, queries_here, value_width):
    maxima = jnp.full((2, heads_here, queries_here), FLOOR, jnp.float32)
    totals = jnp.zeros((2, heads_here, queries_here), jnp.float32)
    sums = jnp.zeros((2, heads_here, queries_here, value_width), jnp.float32)
    return (maxima, totals, sums)


def absorb_keys(states, queries, keys, values, width):
    maxima, totals, sums = states
    scaling = width ** (-0.5)
    new_maxima = []
    new_totals = []
    new_sums = []
    for which in range(2):
        query_part = queries[:, :, which * width : (which + 1) * width]
        key_part = keys[:, :, which * width : (which + 1) * width]
        scores = (
            jnp.einsum("qhd,khd->hqk", query_part, key_part, preferred_element_type=jnp.float32)
            * scaling
        )
        highest = jnp.maximum(maxima[which], jnp.max(scores, axis=2))
        expo = jnp.exp(scores - highest[:, :, None])
        factor = jnp.exp(maxima[which] - highest)
        new_totals.append(totals[which] * factor + jnp.sum(expo, axis=2))
        carried = jnp.einsum(
            "hqk,khv->hqv", expo.astype(jnp.bfloat16), values, preferred_element_type=jnp.float32
        )
        new_sums.append(sums[which] * factor[:, :, None] + carried)
        new_maxima.append(highest)
    return (jnp.stack(new_maxima), jnp.stack(new_totals), jnp.stack(new_sums))


def finish(states, lambda_row, gain):
    maxima, totals, sums = states
    heard = sums / totals[:, :, :, None]
    differ = heard[0] - lambda_row[:, None, None] * heard[1]
    scaled = lax.rsqrt(jnp.mean(differ * differ, axis=2, keepdims=True) + EPSILON)
    return (differ * scaled * gain).astype(jnp.bfloat16)


def gated_units(grid, w_gate, w_up):
    gate = jnp.einsum("necd,edf->necf", grid, w_gate, preferred_element_type=jnp.float32)
    upward = jnp.einsum("necd,edf->necf", grid, w_up, preferred_element_type=jnp.float32)
    clamped = jnp.minimum(gate, LIMIT)
    return (
        clamped * jax.nn.sigmoid(SLOPE * clamped) * (jnp.clip(upward, -LIMIT, LIMIT) + 1.0)
    ).astype(jnp.bfloat16)


def per_device(
    query_a,
    key_a,
    value_a,
    query_b,
    key_b,
    value_b,
    lambdas,
    gain_a,
    gain_b,
    out_a,
    out_b,
    residual,
    norm_gain,
    route_ids,
    route_weights,
    w_gate,
    w_up,
    w_down,
):
    heads_here = query_a.shape[1]
    queries_here = query_a.shape[0]
    width_a = query_a.shape[2] // 2
    width_b = query_b.shape[2] // 2
    starting = (
        empty_state(heads_here, queries_here, value_a.shape[2]),
        empty_state(heads_here, queries_here, value_b.shape[2]),
    )
    keys_a = lax.all_gather(key_a, "sp", axis=0, tiled=True)
    values_a = lax.all_gather(value_a, "sp", axis=0, tiled=True)
    keys_b = lax.all_gather(key_b, "sp", axis=0, tiled=True)
    values_b = lax.all_gather(value_b, "sp", axis=0, tiled=True)
    state_a = absorb_keys(starting[0], query_a, keys_a, values_a, width_a)
    state_b = absorb_keys(starting[1], query_b, keys_b, values_b, width_b)
    attended_a = finish(state_a, lambdas[0], gain_a)
    attended_b = finish(state_b, lambdas[1], gain_b)
    model_width = out_a.shape[1]
    weights_a = out_a.reshape(heads_here, -1, model_width)
    weights_b = out_b.reshape(heads_here, -1, model_width)
    first = jnp.einsum("hqv,hvd->qd", attended_a, weights_a, preferred_element_type=jnp.float32)
    projected = lax.psum_scatter(
        (
            first
            + jnp.einsum("hqv,hvd->qd", attended_b, weights_b, preferred_element_type=jnp.float32)
        ).astype(jnp.bfloat16),
        "tp",
        scatter_dimension=0,
        tiled=True,
    ).astype(jnp.float32)
    mixed = (residual.astype(jnp.float32) + projected).astype(jnp.bfloat16)
    widened = mixed.astype(jnp.float32)
    normed = (
        widened
        * lax.rsqrt(jnp.mean(widened * widened, axis=1, keepdims=True) + EPSILON)
        * norm_gain
    ).astype(jnp.bfloat16)
    rows_here, chosen = route_ids.shape
    groups = lax.axis_size("sp")
    experts_here = w_gate.shape[0]
    experts_all = experts_here * groups
    capacity = 2 * rows_here * chosen // experts_all
    slots_here = experts_here * capacity
    flat_ids = route_ids.reshape(-1)
    onehot = (flat_ids[:, None] == jnp.arange(experts_all, dtype=jnp.int32)[None, :]).astype(
        jnp.int32
    )
    earlier = jnp.cumsum(onehot, axis=0) - onehot
    target = flat_ids * capacity + jnp.sum(earlier * onehot, axis=1)
    places = jnp.arange(experts_all * capacity, dtype=jnp.int32)
    layout = jnp.any(target.reshape(rows_here, chosen)[None, :, :] == places[:, None, None], axis=2)
    outgoing = jnp.dot(
        layout.astype(jnp.bfloat16), normed, preferred_element_type=jnp.float32
    ).astype(jnp.bfloat16)
    outgoing = outgoing.reshape(groups, slots_here, model_width)
    arrived = lax.all_to_all(outgoing, "sp", split_axis=0, concat_axis=0, tiled=True)
    pieces = lax.all_gather(arrived, "tp", axis=0, tiled=True)
    count = pieces.shape[0]
    grid = pieces.reshape(count, experts_here, capacity, model_width)
    active = gated_units(grid, w_gate, w_up)
    down = jnp.einsum("necf,efd->necd", active, w_down, preferred_element_type=jnp.float32)
    partial_value = down.astype(jnp.bfloat16).reshape(count, slots_here, model_width)
    totals = lax.psum_scatter(
        partial_value.astype(jnp.float32).astype(jnp.bfloat16),
        "tp",
        scatter_dimension=0,
        tiled=True,
    )
    summed = lax.all_to_all(totals, "sp", split_axis=0, concat_axis=0, tiled=True)
    results = summed.reshape(experts_all * capacity, model_width)
    picked = (
        jnp.take(results, target, axis=0)
        .reshape(rows_here, chosen, model_width)
        .astype(jnp.float32)
    )
    combined = jnp.sum(route_weights[:, :, None] * picked, axis=1)
    return (widened + combined).astype(jnp.bfloat16)


def solution(mesh):
    in_specs = (
        P("sp", "tp", None),
        P("sp", "tp", None),
        P("sp", "tp", None),
        P("sp", "tp", None),
        P("sp", "tp", None),
        P("sp", "tp", None),
        P(None, "tp"),
        P(),
        P(),
        P("tp", None),
        P("tp", None),
        P(("sp", "tp"), None),
        P(),
        P(("sp", "tp"), None),
        P(("sp", "tp"), None),
        P("sp", None, "tp"),
        P("sp", None, "tp"),
        P("sp", "tp", None),
    )
    out_specs = P(("sp", "tp"), None)
    return jax.shard_map(
        per_device, mesh=mesh, in_specs=in_specs, out_specs=out_specs, check_vma=False
    )
```

profile of v0, /device:TPU:0, one launch (start us, length us, event | category | flops | bytes accessed | tf_op | source)
XLA Modules:
  0.0 234.9 jit_solution(8185951982461286773)
XLA Ops:
  6.5 1.1 copy.77
  7.6 11.5 %all_gather.15 = bf16[512,2,256]{2,0,1:T(8,128)(2,1)S(1)} all-gather(bf16[128,2,256]{2,0,1:T(8,128)(2,1)S(1)} %copy.77), channel_id=1, replica_groups=mesh['sp'=4,'tp'=8] {'sp'}, dimensions={0}, use_global_device_ids=true | all-gather | bytes 655360 | tf_op jit(solution)/shard_map/all_gather | solution.py:89
  19.1 1.0 fusion.120
  20.1 0.0 copy-start.6
  20.2 0.3 fusion.125
  20.5 0.3 fusion.124
  20.8 1.0 copy.78
  21.8 10.2 %all_gather.16 = bf16[512,2,256]{2,0,1:T(8,128)(2,1)S(1)} all-gather(bf16[128,2,256]{2,0,1:T(8,128)(2,1)S(1)} %copy.78), channel_id=1, replica_groups=mesh['sp'=4,'tp'=8] {'sp'}, dimensions={0}, use_global_device_ids=true | all-gather | bytes 655360 | tf_op jit(solution)/shard_map/all_gather | solution.py:90
  31.9 0.2 fusion.59
  32.2 0.2 fusion.61
  32.4 0.3 fusion.50
  32.7 0.3 fusion.49
  33.0 0.0 copy-start.14
  33.1 0.1 maximum_divide_fusion
  33.2 0.8 copy-done.2
  34.0 0.2 fusion.79
  34.2 0.1 copy.81
  34.3 8.6 %all_gather.17 = bf16[512,2,128]{0,2,1:T(8,128)(2,1)S(1)} all-gather(bf16[128,2,128]{0,2,1:T(8,128)(2,1)S(1)} %copy.81), channel_id=1, replica_groups=mesh['sp'=4,'tp'=8] {'sp'}, dimensions={0}, use_global_device_ids=true | all-gather | bytes 327680 | tf_op jit(solution)/shard_map/all_gather | solution.py:91
  42.9 0.1 fusion.121
  43.0 0.3 fusion.123
  43.3 0.3 fusion.122
  43.6 0.1 copy.82
  43.8 0.0 copy-start.1
  43.8 9.0 %all_gather.18 = bf16[512,2,128]{0,2,1:T(8,128)(2,1)S(1)} all-gather(bf16[128,2,128]{0,2,1:T(8,128)(2,1)S(1)} %copy.82), channel_id=1, replica_groups=mesh['sp'=4,'tp'=8] {'sp'}, dimensions={0}, use_global_device_ids=true | all-gather | bytes 327680 | tf_op jit(solution)/shard_map/all_gather | solution.py:92
  52.8 0.2 fusion.63
  53.1 0.2 fusion.65
  53.3 0.3 fusion.52
  53.6 0.3 fusion.51
  54.0 0.1 fusion.96
  54.1 0.6 convolution_bitcast_fusion
  54.7 0.0 copy-start.10
  54.7 1.8 fusion.2
  56.6 0.0 reduce-scatter.3.cloned.1.call-update
  56.6 0.0 all-gather.2.cloned.1.call-start
  56.7 0.1 copy.86
  56.7 0.1 reshape.254
  56.8 0.1 fusion.111
  56.9 0.1 reduce_window_sum.11
  57.0 0.2 select_reduce_fusion
  57.1 0.1 reduce_sum.104
  57.2 0.1 copy.87
  57.3 0.1 fusion.112
  57.4 32.2 %reduce-scatter.3.cloned.1.call-done = bf16[16,4096]{1,0:T(8,128)(2,1)} async-done(((bf16[128,4096]{1,0:T(8,128)(2,1)}), bf16[16,4096]{1,0:T(8,128)(2,1)}) %reduce-scatter.3.cloned.1.call-update) | async-done | bytes 131088 | tf_op jit(solution)/shard_map/reduce_scatter | solution.py:101
  89.6 1.1 fusion.67
  90.7 1.2 convolution_convert_fusion.1
  91.9 11.0 %all_to_all.10 = bf16[4,16,4096]{2,1,0:T(8,128)(2,1)} all-to-all(bf16[4,16,4096]{2,1,0:T(8,128)(2,1)S(1)} %bitcast.129), channel_id=1, replica_groups=mesh['sp'=4,'tp'=8] {'sp'}, dimensions={0} | all-to-all | bytes 1048576 | tf_op jit(solution)/shard_map/all_to_all | solution.py:135
  102.9 0.0 all-gather.2.cloned.1.call-update
  102.9 0.0 reduce-scatter.5.cloned.1.call-start
  103.0 45.4 %all-gather.2.cloned.1.call-done = bf16[32,16,4096]{2,1,0:T(8,128)(2,1)} async-done(((bf16[4,16,4096]{2,1,0:T(8,128)(2,1)}), bf16[32,16,4096]{2,1,0:T(8,128)(2,1)}) %all-gather.2.cloned.1.call-update) | async-done | bytes 4194320 | tf_op jit(solution)/shard_map/all_gather | solution.py:136
  148.3 4.7 %fusion.15 = f32[32,2,8,256]{3,2,0,1:T(8,128)S(1)} fusion(bf16[2,4096,256]{2,1,0:T(8,128)(2,1)} %param.33, bf16[32,16,4096]{2,1,0:T(8,128)(2,1)} %all-gather.2.cloned.1.call-done), kind=kOutput, calls=%fused_computation.21 | convolution fusion | flops 1073872896 | bytes 8912896 | tf_op jit(solution)/shard_map/necd,edf->necf/dot_general | solution.py:53
  153.1 9.1 %fusion = bf16[32,2,8,4096]{3,2,0,1:T(8,128)(2,1)} fusion(bf16[2,256,4096]{2,1,0:T(8,128)(2,1)} %param.35, bf16[2,4096,256]{2,1,0:T(8,128)(2,1)} %param.34, f32[32,2,8,256]{3,2,0,1:T(8,128)S(1)} %fusion.15, bf16[32,16,4096]{2,1,0:T(8,128)(2,1)} %all-gather.2.cloned.1.call-done), kind=kOutput, calls=%fused_computation.2 | convolution fusion | flops 2150760448 | bytes 17301504 | tf_op jit(solution)/shard_map/necf,efd->necd/dot_general | solution.py:140
  162.2 4.6 %copy.138 = bf16[32,2,8,4096]{3,2,1,0:T(8,128)(2,1)} copy(bf16[32,2,8,4096]{3,2,0,1:T(8,128)(2,1)} %fusion) | data formatting | bytes 8388608 | tf_op jit(solution)/shard_map/convert_element_type | solution.py:141
  166.8 0.0 reduce-scatter.5.cloned.1.call-update
  166.8 48.9 %reduce-scatter.5.cloned.1.call-done = bf16[4,16,4096]{2,1,0:T(8,128)(2,1)} async-done(((bf16[32,16,4096]{2,1,0:T(8,128)(2,1)}), bf16[4,16,4096]{2,1,0:T(8,128)(2,1)}) %reduce-scatter.5.cloned.1.call-update) | async-done | bytes 524304 | tf_op jit(solution)/shard_map/reduce_scatter | solution.py:142
  215.7 3.6 %all-to-all-start.1 = ((bf16[4,16,4096]{2,1,0:T(8,128)(2,1)}), bf16[4,16,4096]{2,1,0:T(8,128)(2,1)S(1)}, u32[]{:S(2)}, u32[]{:S(2)}) async-start(bf16[4,16,4096]{2,1,0:T(8,128)(2,1)} %reduce-scatter.5.cloned.1.call-done), calls=%async_computation.3 | async-start | bytes 1048576 | tf_op jit(solution)/shard_map/all_to_all | solution.py:148
  219.3 0.1 copy.92
  219.4 0.1 mul.208
  219.5 0.1 copy.88
  219.6 0.1 copy.85
  219.7 6.2 %all-to-all-done.1 = bf16[4,16,4096]{2,1,0:T(8,128)(2,1)S(1)} async-done(((bf16[4,16,4096]{2,1,0:T(8,128)(2,1)}), bf16[4,16,4096]{2,1,0:T(8,128)(2,1)S(1)}, u32[]{:S(2)}, u32[]{:S(2)}) %all-to-all-start.1) | async-done | bytes 524320 | tf_op jit(solution)/shard_map/all_to_all | solution.py:148
  225.9 0.7 gather_fusion
  226.6 0.2 gather.7
  226.8 0.8 multiply_reduce_fusion
  227.7 0.7 fusion.70
  (43 shorter events, 0.2 us)
Async XLA Ops:
  6.5 47.6 %copy-start = (bf16[256,4096]{1,0:T(8,128)(2,1)S(1)}, bf16[256,4096]{1,0:T(8,128)(2,1)}, u32[]{:S(2)}) copy-start(bf16[256,4096]{1,0:T(8,128)(2,1)} %param.28) | copy-start | bytes 6291460
  6.5 26.5 %copy-start.13 = (f32[2,2]{1,0:T(2,128)S(1)}, f32[2,2]{1,0:T(2,128)}, u32[]{:S(2)}) copy-start(f32[2,2]{1,0:T(2,128)} %param.24) | copy-start | bytes 52
  6.5 83.1 %reduce-scatter.3.cloned.1.call-start = ((), (), s32[]{:S(2)}) async-start(), calls=%async_computation.4 | async-start | bytes 1179648 | tf_op jit(solution)/shard_map/reduce_scatter | solution.py:101
  19.1 15.1 %copy-start.7 = (bf16[128,2,128]{2,1,0:T(2,128)(2,1)S(1)}, bf16[128,2,128]{2,1,0:T(2,128)(2,1)}, u32[]{:S(2)}) copy-start(bf16[128,2,128]{2,1,0:T(2,128)(2,1)} %param.22) | copy-start | bytes 196612
  20.1 22.8 %copy-start.6 = (bf16[128,2,128]{2,1,0:T(2,128)(2,1)S(1)}, bf16[128,2,128]{2,1,0:T(2,128)(2,1)}, u32[]{:S(2)}) copy-start(bf16[128,2,128]{2,1,0:T(2,128)(2,1)} %param.21) | copy-start | bytes 196612
  20.8 22.8 %copy-start.8 = (bf16[128,2,128]{2,1,0:T(2,128)(2,1)S(1)}, bf16[128,2,128]{2,1,0:T(2,128)(2,1)}, u32[]{:S(2)}) copy-start(bf16[128,2,128]{2,1,0:T(2,128)(2,1)} %param.23) | copy-start | bytes 196612
  33.0 21.1 %copy-start.14 = (f32[128]{0:T(128)S(1)}, f32[128]{0:T(128)}, u32[]{:S(2)}) copy-start(f32[128]{0:T(128)} %param.26) | copy-start | bytes 1540
  33.2 0.8 copy-start.2
  43.8 10.9 %copy-start.1 = (bf16[512,4096]{1,0:T(8,128)(2,1)S(1)}, bf16[512,4096]{1,0:T(8,128)(2,1)}, u32[]{:S(2)}) copy-start(bf16[512,4096]{1,0:T(8,128)(2,1)} %param.27) | copy-start | bytes 12582916
  43.8 10.9 %copy-start.3 = (f32[2,2,128,256]{3,2,1,0:T(8,128)S(1)}, f32[2,2,128,256]{3,2,1,0:T(8,128)}, u32[]{:S(2)}) copy-start(f32[2,2,128,256]{3,2,1,0:T(8,128)} %copy-done.2) | copy-start | bytes 1572868
  43.8 10.9 %copy-start.11 = (f32[256]{0:T(256)S(1)}, f32[256]{0:T(256)}, u32[]{:S(2)}) copy-start(f32[256]{0:T(256)} %param.25) | copy-start | bytes 3076
  54.7 1.9 copy-start.10
  54.7 34.9 %copy-start.4 = (bf16[16,4096]{1,0:T(8,128)(2,1)S(1)}, bf16[16,4096]{1,0:T(8,128)(2,1)}, u32[]{:S(2)}) copy-start(bf16[16,4096]{1,0:T(8,128)(2,1)} %param.29) | copy-start | bytes 393220
  54.7 35.9 %copy-start.9 = (f32[4096]{0:T(1024)S(1)}, f32[4096]{0:T(1024)}, u32[]{:S(2)}) copy-start(f32[4096]{0:T(1024)} %param.30) | copy-start | bytes 49156
  56.6 91.7 %all-gather.2.cloned.1.call-start = ((), (), s32[]{:S(2)}) async-start(), calls=%async_computation.5 | async-start | bytes 4718592 | tf_op jit(solution)/shard_map/all_gather | solution.py:136
  102.9 112.8 %reduce-scatter.5.cloned.1.call-start = ((), (), s32[]{:S(2)}) async-start(), calls=%async_computation.6 | async-start | bytes 4718592 | tf_op jit(solution)/shard_map/reduce_scatter | solution.py:142
  166.8 52.8 %copy-start.12 = (f32[16,2]{0,1:T(2,128)S(1)}, f32[16,2]{0,1:T(2,128)}, u32[]{:S(2)}) copy-start(f32[16,2]{0,1:T(2,128)} %param.32) | copy-start | bytes 388
  166.8 60.9 %copy-start.5 = (bf16[16,4096]{1,0:T(8,128)(2,1)S(1)}, bf16[16,4096]{1,0:T(8,128)(2,1)}, u32[]{:S(2)}) copy-start(bf16[16,4096]{1,0:T(8,128)(2,1)} %reduce-scatter.3.cloned.1.call-done) | copy-start | bytes 393220
  215.7 10.2 %all-to-all-start.1 = ((bf16[4,16,4096]{2,1,0:T(8,128)(2,1)}), bf16[4,16,4096]{2,1,0:T(8,128)(2,1)S(1)}, u32[]{:S(2)}, u32[]{:S(2)}) async-start(bf16[4,16,4096]{2,1,0:T(8,128)(2,1)} %reduce-scatter.5.cloned.1.call-done), calls=%async_computation.3 | async-start | bytes 1048576 | tf_op jit(solution)/shard_map/all_to_all | solution.py:148
Sparse Core Ops, SparseCore 0:
  56.7 32.8 reduce-scatter.2
  103.0 45.2 all-gather.1
  166.9 48.7 reduce-scatter.4
where the time goes:
time: 235 us
  waiting for transfers between devices  133 us (57%)
  blocking collectives  50.2 us (21%)
  matrix products  19.9 us (8%)
  between operations  13.5 us (6%)
  local copies, waits for them, and re-layouts  10.5 us (4%)
  other arithmetic  4.46 us (2%)
  starting transfers between devices  3.72 us (2%)
    reduce_scatter x1, waiting for transfers between devices, per_device(): lax.psum_scatter(partial_value.astype(jnp.float32).astype(jnp.bfloat16),...  48.9 us
    all_gather x1, waiting for transfers between devices, per_device(): pieces = lax.all_gather(arrived, 'tp', axis=0, tiled=True)  45.4 us
    reduce_scatter x1, waiting for transfers between devices, per_device(): lax.psum_scatter((first + jnp.einsum('hqv,hvd->qd', attended_b, weights_b...  32.2 us
    all_gather x1, blocking collectives, per_device(): keys_a = lax.all_gather(key_a, 'sp', axis=0, tiled=True)  11.5 us
    all_to_all x1, blocking collectives, per_device(): lax.all_to_all(outgoing, 'sp', split_axis=0, concat_axis=0, tiled=True)  11 us
    all_gather x1, blocking collectives, per_device(): values_a = lax.all_gather(value_a, 'sp', axis=0, tiled=True)  10.2 us
    dot_general x1, matrix products, per_device(): jnp.einsum('necf,efd->necd', active, w_down, preferred_element_type=jnp.f...  9.1 us
    all_gather x1, blocking collectives, per_device(): values_b = lax.all_gather(value_b, 'sp', axis=0, tiled=True)  9.03 us
  transfers between devices with their start and end apart: 4, of which 4 were waited for; matrix products, arithmetic and copies ran while one was open for 0% of the time, Pallas kernels for 0%

commit v1 on v0

--- a/solution.py
+++ b/solution.py
@@ -7,6 +7,18 @@
 LIMIT = 7.0
 SLOPE = 1.702
 FLOOR = -1e30
+
+
+def bring_the_array(row_data, ax_name):
+    devs = lax.psum(1, ax_name)
+    queue = [(p, (p + 1) % devs) for p in range(devs)]
+    small = [None] * devs
+    small[devs - 1] = row_data
+    for it in range(devs - 2, -1, -1):
+        small[it] = lax.ppermute(small[it + 1], ax_name, queue)
+    k_now = jnp.concatenate(small, axis=0)
+    block_next = (lax.axis_index(ax_name) + 1) * row_data.shape[0]
+    return jnp.roll(k_now, block_next, axis=0)
 
 
 def empty_state(heads_here, queries_here, value_width):
@@ -133,7 +145,7 @@
     ).astype(jnp.bfloat16)
     outgoing = outgoing.reshape(groups, slots_here, model_width)
     arrived = lax.all_to_all(outgoing, "sp", split_axis=0, concat_axis=0, tiled=True)
-    pieces = lax.all_gather(arrived, "tp", axis=0, tiled=True)
+    pieces = bring_the_array(arrived, "tp")
     count = pieces.shape[0]
     grid = pieces.reshape(count, experts_here, capacity, model_width)
     active = gated_units(grid, w_gate, w_up)

time: 235 us -> 275 us (1.17)
  waiting for transfers between devices: 133 us -> 158 us
  local copies, waits for them, and re-layouts: 10.5 us -> 27.8 us
  matrix products: 19.9 us -> 16.3 us
    ppermute x0 -> x7, waiting for transfers between devices: none -> 73.2 us  [bring_the_array(): small[it] = lax.ppermute(small[it + 1], ax_name, queue)]
    all_gather x1 -> x0, waiting for transfers between devices: 45.4 us -> none  [per_device(): pieces = lax.all_gather(arrived, 'tp', axis=0, tiled=True)]
    unnamed x36 -> x61, local copies, waits for them, and re-layouts: 3.29 us -> 18.6 us
    dot_general x1, matrix products: 4.71 us -> 1.25 us  [gated_units(): jnp.einsum('necd,edf->necf', grid, w_gate, preferred_element_type=jnp.flo...]
  transfers between devices with their start and end apart: 4 -> 10, of which waited for: 4 -> 10; matrix products, arithmetic and copies ran while one was open for 0% -> 0% of each run, Pallas kernels for 0% -> 0%
where the time goes in v1:
time: 275 us; the launch traced here: 274 us
  waiting for transfers between devices  158 us (57%)
  blocking collectives  49.3 us (18%)
  local copies, waits for them, and re-layouts  27.8 us (10%)
  matrix products  16.3 us (6%)
  between operations  13.9 us (5%)
  other arithmetic  4.43 us (2%)
  starting transfers between devices  3.71 us (1%)
    ppermute x7, waiting for transfers between devices, bring_the_array(): small[it] = lax.ppermute(small[it + 1], ax_name, queue)  73.2 us
    reduce_scatter x1, waiting for transfers between devices, per_device(): lax.psum_scatter(partial_value.astype(jnp.float32).astype(jnp.bfloat16),...  46.8 us
    reduce_scatter x1, waiting for transfers between devices, per_device(): lax.psum_scatter((first + jnp.einsum('hqv,hvd->qd', attended_b, weights_b...  32.2 us
    unnamed x61, local copies, waits for them, and re-layouts  18.6 us
    all_to_all x1, blocking collectives, per_device(): lax.all_to_all(outgoing, 'sp', split_axis=0, concat_axis=0, tiled=True)  10.5 us
    all_gather x1, blocking collectives, per_device(): keys_b = lax.all_gather(key_b, 'sp', axis=0, tiled=True)  10.5 us
    all_gather x1, blocking collectives, per_device(): keys_a = lax.all_gather(key_a, 'sp', axis=0, tiled=True)  9.74 us
    all_gather x1, blocking collectives, per_device(): values_a = lax.all_gather(value_a, 'sp', axis=0, tiled=True)  9.66 us
  transfers between devices with their start and end apart: 10, of which 10 were waited for; matrix products, arithmetic and copies ran while one was open for 0% of the time, Pallas kernels for 0%

profile of v1, /device:TPU:0, one launch (start us, length us, event | category | flops | bytes accessed | tf_op | source)
XLA Modules:
  0.0 273.8 jit_solution(1752320583373839860)
XLA Ops:
  6.5 1.1 copy.66
  7.7 10.5 %all_gather.14 = bf16[512,2,128]{0,2,1:T(8,128)(2,1)S(1)} all-gather(bf16[128,2,128]{0,2,1:T(8,128)(2,1)S(1)} %copy.66), channel_id=1, replica_groups=mesh['sp'=4,'tp'=8] {'sp'}, dimensions={0}, use_global_device_ids=true | all-gather | bytes 327680 | tf_op jit(solution)/shard_map/all_gather | solution.py:103
  18.1 1.1 fusion.109
  19.2 0.3 fusion.111
  19.5 0.3 fusion.110
  19.8 1.0 copy.67
  20.8 9.0 %all_gather.15 = bf16[512,2,128]{0,2,1:T(8,128)(2,1)S(1)} all-gather(bf16[128,2,128]{0,2,1:T(8,128)(2,1)S(1)} %copy.67), channel_id=1, replica_groups=mesh['sp'=4,'tp'=8] {'sp'}, dimensions={0}, use_global_device_ids=true | all-gather | bytes 327680 | tf_op jit(solution)/shard_map/all_gather | solution.py:104
  29.7 0.2 fusion.43
  30.0 0.2 fusion.45
  30.2 0.3 fusion.38
  30.5 0.3 fusion.37
  30.9 1.1 slice_bitcast_fusion.1
  32.0 0.1 fusion.84
  32.1 0.9 copy.62
  33.0 9.7 %all_gather.12 = bf16[512,2,256]{2,0,1:T(8,128)(2,1)S(1)} all-gather(bf16[128,2,256]{2,0,1:T(8,128)(2,1)S(1)} %copy.62), channel_id=1, replica_groups=mesh['sp'=4,'tp'=8] {'sp'}, dimensions={0}, use_global_device_ids=true | all-gather | bytes 655360 | tf_op jit(solution)/shard_map/all_gather | solution.py:101
  42.8 1.0 fusion.108
  43.7 0.3 fusion.113
  44.0 0.3 fusion.112
  44.4 9.7 %all_gather.13 = bf16[512,2,256]{2,0,1:T(8,128)(2,1)S(1)} all-gather(bf16[128,2,256]{2,0,1:T(8,128)(2,1)S(1)} %copy.63), channel_id=1, replica_groups=mesh['sp'=4,'tp'=8] {'sp'}, dimensions={0}, use_global_device_ids=true | all-gather | bytes 655360 | tf_op jit(solution)/shard_map/all_gather | solution.py:102
  54.1 0.2 fusion.39
  54.3 0.2 fusion.41
  54.5 0.3 fusion.36
  54.9 0.3 fusion.35
  55.2 0.1 maximum_divide_fusion
  55.3 0.2 fusion.67
  55.5 0.6 convolution_bitcast_fusion
  56.1 1.8 fusion.2
  58.3 0.2 select_reduce_fusion
  58.5 0.1 copy.72
  58.7 32.2 %reduce-scatter.3.cloned.1.call-done = bf16[16,4096]{1,0:T(8,128)(2,1)} async-done(((bf16[128,4096]{1,0:T(8,128)(2,1)}), bf16[16,4096]{1,0:T(8,128)(2,1)}) %reduce-scatter.3.cloned.1.call-update) | async-done | bytes 131088 | tf_op jit(solution)/shard_map/reduce_scatter | solution.py:113
  91.0 1.1 fusion.47
  92.0 1.3 convolution_convert_fusion.1
  93.3 10.5 %all_to_all.10 = bf16[4,16,4096]{2,1,0:T(8,128)(2,1)S(1)} all-to-all(bf16[4,16,4096]{2,1,0:T(8,128)(2,1)S(1)} %bitcast.124), channel_id=1, replica_groups=mesh['sp'=4,'tp'=8] {'sp'}, dimensions={0} | all-to-all | bytes 1048576 | tf_op jit(solution)/shard_map/all_to_all | solution.py:147
  103.8 10.4 %collective-permute-done = bf16[4,16,4096]{2,1,0:T(8,128)(2,1)S(1)} collective-permute-done((bf16[4,16,4096]{2,1,0:T(8,128)(2,1)S(1)}, bf16[4,16,4096]{2,1,0:T(8,128)(2,1)S(1)}, u32[]{:S(2)}, u32[]{:S(2)}) %collective-permute-start) | collective-permute-done | bytes 524320 | tf_op jit(solution)/shard_map/ppermute | solution.py:18
  114.2 10.4 %collective-permute-done.1 = bf16[4,16,4096]{2,1,0:T(8,128)(2,1)S(1)} collective-permute-done((bf16[4,16,4096]{2,1,0:T(8,128)(2,1)S(1)}, bf16[4,16,4096]{2,1,0:T(8,128)(2,1)S(1)}, u32[]{:S(2)}, u32[]{:S(2)}) %collective-permute-start.1) | collective-permute-done | bytes 524320 | tf_op jit(solution)/shard_map/ppermute | solution.py:18
  124.6 0.8 copy-done.2
  125.4 10.4 %collective-permute-done.2 = bf16[4,16,4096]{2,1,0:T(8,128)(2,1)S(1)} collective-permute-done((bf16[4,16,4096]{2,1,0:T(8,128)(2,1)S(1)}, bf16[4,16,4096]{2,1,0:T(8,128)(2,1)S(1)}, u32[]{:S(2)}, u32[]{:S(2)}) %collective-permute-start.2) | collective-permute-done | bytes 524320 | tf_op jit(solution)/shard_map/ppermute | solution.py:18
  135.8 0.8 copy-done.4
  136.6 10.4 %collective-permute-done.3 = bf16[4,16,4096]{2,1,0:T(8,128)(2,1)S(1)} collective-permute-done((bf16[4,16,4096]{2,1,0:T(8,128)(2,1)S(1)}, bf16[4,16,4096]{2,1,0:T(8,128)(2,1)S(1)}, u32[]{:S(2)}, u32[]{:S(2)}) %collective-permute-start.3) | collective-permute-done | bytes 524320 | tf_op jit(solution)/shard_map/ppermute | solution.py:18
  147.0 0.8 copy-done.6
  147.8 10.4 %collective-permute-done.4 = bf16[4,16,4096]{2,1,0:T(8,128)(2,1)S(1)} collective-permute-done((bf16[4,16,4096]{2,1,0:T(8,128)(2,1)S(1)}, bf16[4,16,4096]{2,1,0:T(8,128)(2,1)S(1)}, u32[]{:S(2)}, u32[]{:S(2)}) %collective-permute-start.4) | collective-permute-done | bytes 524320 | tf_op jit(solution)/shard_map/ppermute | solution.py:18
  158.2 0.8 copy-done.8
  159.1 10.5 %collective-permute-done.5 = bf16[4,16,4096]{2,1,0:T(8,128)(2,1)} collective-permute-done((bf16[4,16,4096]{2,1,0:T(8,128)(2,1)S(1)}, bf16[4,16,4096]{2,1,0:T(8,128)(2,1)}, u32[]{:S(2)}, u32[]{:S(2)}) %collective-permute-start.5) | collective-permute-done | bytes 524320 | tf_op jit(solution)/shard_map/ppermute | solution.py:18
  169.6 10.7 %collective-permute-done.6 = bf16[4,16,4096]{2,1,0:T(8,128)(2,1)} collective-permute-done((bf16[4,16,4096]{2,1,0:T(8,128)(2,1)}, bf16[4,16,4096]{2,1,0:T(8,128)(2,1)}, u32[]{:S(2)}, u32[]{:S(2)}) %collective-permute-start.6) | collective-permute-done | bytes 524320 | tf_op jit(solution)/shard_map/ppermute | solution.py:18
  180.3 1.1 constant_dynamic-update-slice_fusion.15
  181.4 1.1 constant_dynamic-update-slice_fusion.14
  182.4 1.1 constant_dynamic-update-slice_fusion.13
  183.5 1.1 constant_dynamic-update-slice_fusion.12
  184.6 1.1 constant_dynamic-update-slice_fusion.11
  185.7 1.1 constant_dynamic-update-slice_fusion.10
  186.9 1.1 constant_dynamic-update-slice_fusion.7
  187.9 1.1 constant_dynamic-update-slice_fusion.6
  189.3 3.2 %copy-done.13 = bf16[64,16,4096]{2,1,0:T(8,128)(2,1)} copy-done((bf16[64,16,4096]{2,1,0:T(8,128)(2,1)}, bf16[64,16,4096]{2,1,0:T(8,128)(2,1)S(1)}, u32[]{:S(2)}) %copy-start.13) | copy-done | bytes 8388632
  192.6 1.3 fusion.15
  193.8 9.1 %fusion = bf16[32,2,8,4096]{3,2,0,1:T(8,128)(2,1)} fusion(bf16[2,256,4096]{2,1,0:T(8,128)(2,1)} %param.35, f32[32,2,8,256]{3,2,0,1:T(8,128)S(1)} %fusion.15, bf16[2,4096,256]{2,1,0:T(8,128)(2,1)} %param.34, bf16[64,16,4096]{2,1,0:T(8,128)(2,1)} %copy-done.13, s32[]{:T(128)S(6)} %select_n.37), kind=kOutput, calls=%fused_computation.2 | convolution fusion | flops 2150760448 | bytes 17301508 | tf_op jit(solution)/shard_map/necf,efd->necd/dot_general | solution.py:152
  202.9 4.6 %copy.121 = bf16[32,2,8,4096]{3,2,1,0:T(8,128)(2,1)} copy(bf16[32,2,8,4096]{3,2,0,1:T(8,128)(2,1)} %fusion) | data formatting | bytes 8388608 | tf_op jit(solution)/shard_map/convert_element_type | solution.py:153
  207.6 46.8 %reduce-scatter.5.cloned.1.call-done = bf16[4,16,4096]{2,1,0:T(8,128)(2,1)} async-done(((bf16[32,16,4096]{2,1,0:T(8,128)(2,1)}), bf16[4,16,4096]{2,1,0:T(8,128)(2,1)}) %reduce-scatter.5.cloned.1.call-update) | async-done | bytes 524304 | tf_op jit(solution)/shard_map/reduce_scatter | solution.py:154
  254.3 3.7 %all-to-all-start.1 = ((bf16[4,16,4096]{2,1,0:T(8,128)(2,1)}), bf16[4,16,4096]{2,1,0:T(8,128)(2,1)S(1)}, u32[]{:S(2)}, u32[]{:S(2)}) async-start(bf16[4,16,4096]{2,1,0:T(8,128)(2,1)} %reduce-scatter.5.cloned.1.call-done), calls=%async_computation.3 | async-start | bytes 1048576 | tf_op jit(solution)/shard_map/all_to_all | solution.py:160
  258.2 0.1 copy.73
  258.4 6.2 %all-to-all-done.1 = bf16[4,16,4096]{2,1,0:T(8,128)(2,1)S(1)} async-done(((bf16[4,16,4096]{2,1,0:T(8,128)(2,1)}), bf16[4,16,4096]{2,1,0:T(8,128)(2,1)S(1)}, u32[]{:S(2)}, u32[]{:S(2)}) %all-to-all-start.1) | async-done | bytes 524320 | tf_op jit(solution)/shard_map/all_to_all | solution.py:160
  264.6 0.7 gather_fusion
  265.3 0.2 gather.7
  265.5 0.8 multiply_reduce_fusion
  266.3 0.7 fusion.50
  (80 shorter events, 1.3 us)
Async XLA Ops:
  6.5 49.0 %copy-start = (bf16[256,4096]{1,0:T(8,128)(2,1)S(1)}, bf16[256,4096]{1,0:T(8,128)(2,1)}, u32[]{:S(2)}) copy-start(bf16[256,4096]{1,0:T(8,128)(2,1)} %param.28) | copy-start | bytes 6291460
  6.5 37.8 %copy-start.12 = (bf16[128,2,256]{2,1,0:T(2,128)(2,1)S(1)}, bf16[128,2,256]{2,1,0:T(2,128)(2,1)}, u32[]{:S(2)}) copy-start(bf16[128,2,256]{2,1,0:T(2,128)(2,1)} %param.20) | copy-start | bytes 393220
  6.5 49.0 %copy-start.18 = (f32[128]{0:T(128)S(1)}, f32[128]{0:T(128)}, u32[]{:S(2)}) copy-start(f32[128]{0:T(128)} %param.26) | copy-start | bytes 1540
  6.5 84.4 %reduce-scatter.3.cloned.1.call-start = ((), (), s32[]{:S(2)}) async-start(), calls=%async_computation.4 | async-start | bytes 1179648 | tf_op jit(solution)/shard_map/reduce_scatter | solution.py:113
  30.0 26.2 %copy-start.1 = (bf16[512,4096]{1,0:T(8,128)(2,1)S(1)}, bf16[512,4096]{1,0:T(8,128)(2,1)}, u32[]{:S(2)}) copy-start(bf16[512,4096]{1,0:T(8,128)(2,1)} %param.27) | copy-start | bytes 12582916
  30.0 26.2 %copy-start.16 = (f32[256]{0:T(256)S(1)}, f32[256]{0:T(256)}, u32[]{:S(2)}) copy-start(f32[256]{0:T(256)} %param.25) | copy-start | bytes 3076
  54.5 3.4 %copy-start.15 = (s32[16,2]{0,1:T(2,128)S(1)}, s32[16,2]{0,1:T(2,128)}, u32[]{:S(2)}) copy-start(s32[16,2]{0,1:T(2,128)} %param.31) | copy-start | bytes 388
  54.5 36.4 %copy-start.10 = (bf16[16,4096]{1,0:T(8,128)(2,1)S(1)}, bf16[16,4096]{1,0:T(8,128)(2,1)}, u32[]{:S(2)}) copy-start(bf16[16,4096]{1,0:T(8,128)(2,1)} %param.29) | copy-start | bytes 393220
  54.9 37.2 %copy-start.14 = (f32[4096]{0:T(1024)S(1)}, f32[4096]{0:T(1024)}, u32[]{:S(2)}) copy-start(f32[4096]{0:T(1024)} %param.30) | copy-start | bytes 49156
  57.9 196.4 %reduce-scatter.5.cloned.1.call-start = ((), (), s32[]{:S(2)}) async-start(), calls=%async_computation.5 | async-start | bytes 4718592 | tf_op jit(solution)/shard_map/reduce_scatter | solution.py:154
  103.8 10.4 %collective-permute-start = (bf16[4,16,4096]{2,1,0:T(8,128)(2,1)S(1)}, bf16[4,16,4096]{2,1,0:T(8,128)(2,1)S(1)}, u32[]{:S(2)}, u32[]{:S(2)}) collective-permute-start(bf16[4,16,4096]{2,1,0:T(8,128)(2,1)S(1)} %all_to_all.10), channel_id=1, source_target_pairs={{0,1},{1,2},{2,3},{3,4},{4,5},{5,6},{6,7},{7,0},{8,9},{9,10},{10,1... | collective-permute-start | bytes 1572872 | tf_op jit(solution)/shard_map/ppermute | solution.py:18
  114.2 10.4 %collective-permute-start.1 = (bf16[4,16,4096]{2,1,0:T(8,128)(2,1)S(1)}, bf16[4,16,4096]{2,1,0:T(8,128)(2,1)S(1)}, u32[]{:S(2)}, u32[]{:S(2)}) collective-permute-start(bf16[4,16,4096]{2,1,0:T(8,128)(2,1)S(1)} %collective-permute-done), channel_id=1, source_target_pairs={{0,1},{1,2},{2,3},{3,4},{4,5},{5,6},{6,7},{7,0},{8,9},{9,10},{10,1... | collective-permute-start | bytes 1572872 | tf_op jit(solution)/shard_map/ppermute | solution.py:18
  124.6 0.8 copy-start.2
  125.4 10.4 %collective-permute-start.2 = (bf16[4,16,4096]{2,1,0:T(8,128)(2,1)S(1)}, bf16[4,16,4096]{2,1,0:T(8,128)(2,1)S(1)}, u32[]{:S(2)}, u32[]{:S(2)}) collective-permute-start(bf16[4,16,4096]{2,1,0:T(8,128)(2,1)S(1)} %collective-permute-done.1), channel_id=1, source_target_pairs={{0,1},{1,2},{2,3},{3,4},{4,5},{5,6},{6,7},{7,0},{8,9},{9,10},{10,1... | collective-permute-start | bytes 1572872 | tf_op jit(solution)/shard_map/ppermute | solution.py:18
  135.8 0.8 copy-start.4
  136.6 10.4 %collective-permute-start.3 = (bf16[4,16,4096]{2,1,0:T(8,128)(2,1)S(1)}, bf16[4,16,4096]{2,1,0:T(8,128)(2,1)S(1)}, u32[]{:S(2)}, u32[]{:S(2)}) collective-permute-start(bf16[4,16,4096]{2,1,0:T(8,128)(2,1)S(1)} %collective-permute-done.2), channel_id=1, source_target_pairs={{0,1},{1,2},{2,3},{3,4},{4,5},{5,6},{6,7},{7,0},{8,9},{9,10},{10,1... | collective-permute-start | bytes 1572872 | tf_op jit(solution)/shard_map/ppermute | solution.py:18
  147.0 0.8 copy-start.6
  147.8 10.4 %collective-permute-start.4 = (bf16[4,16,4096]{2,1,0:T(8,128)(2,1)S(1)}, bf16[4,16,4096]{2,1,0:T(8,128)(2,1)S(1)}, u32[]{:S(2)}, u32[]{:S(2)}) collective-permute-start(bf16[4,16,4096]{2,1,0:T(8,128)(2,1)S(1)} %collective-permute-done.3), channel_id=1, source_target_pairs={{0,1},{1,2},{2,3},{3,4},{4,5},{5,6},{6,7},{7,0},{8,9},{9,10},{10,1... | collective-permute-start | bytes 1572872 | tf_op jit(solution)/shard_map/ppermute | solution.py:18
  158.2 0.8 copy-start.8
  159.1 10.5 %collective-permute-start.5 = (bf16[4,16,4096]{2,1,0:T(8,128)(2,1)S(1)}, bf16[4,16,4096]{2,1,0:T(8,128)(2,1)}, u32[]{:S(2)}, u32[]{:S(2)}) collective-permute-start(bf16[4,16,4096]{2,1,0:T(8,128)(2,1)S(1)} %collective-permute-done.4), channel_id=1, source_target_pairs={{0,1},{1,2},{2,3},{3,4},{4,5},{5,6},{6,7},{7,0},{8,9},{9,10},{10,1... | collective-permute-start | bytes 1572872 | tf_op jit(solution)/shard_map/ppermute | solution.py:18
  169.6 10.7 %collective-permute-start.6 = (bf16[4,16,4096]{2,1,0:T(8,128)(2,1)}, bf16[4,16,4096]{2,1,0:T(8,128)(2,1)}, u32[]{:S(2)}, u32[]{:S(2)}) collective-permute-start(bf16[4,16,4096]{2,1,0:T(8,128)(2,1)} %collective-permute-done.5), channel_id=1, source_target_pairs={{0,1},{1,2},{2,3},{3,4},{4,5},{5,6},{6,7},{7,0},{8,9},{9,10},{10,1... | collective-permute-start | bytes 1572872 | tf_op jit(solution)/shard_map/ppermute | solution.py:18
  169.6 19.5 %copy-start.9 = (bf16[4,16,4096]{2,1,0:T(8,128)(2,1)S(1)}, bf16[4,16,4096]{2,1,0:T(8,128)(2,1)}, u32[]{:S(2)}) copy-start(bf16[4,16,4096]{2,1,0:T(8,128)(2,1)} %copy-done.8) | copy-start | bytes 1572868
  169.6 19.5 %copy-start.7 = (bf16[4,16,4096]{2,1,0:T(8,128)(2,1)S(1)}, bf16[4,16,4096]{2,1,0:T(8,128)(2,1)}, u32[]{:S(2)}) copy-start(bf16[4,16,4096]{2,1,0:T(8,128)(2,1)} %copy-done.6) | copy-start | bytes 1572868
  169.6 19.6 %copy-start.5 = (bf16[4,16,4096]{2,1,0:T(8,128)(2,1)S(1)}, bf16[4,16,4096]{2,1,0:T(8,128)(2,1)}, u32[]{:S(2)}) copy-start(bf16[4,16,4096]{2,1,0:T(8,128)(2,1)} %copy-done.4) | copy-start | bytes 1572868
  169.6 19.6 %copy-start.3 = (bf16[4,16,4096]{2,1,0:T(8,128)(2,1)S(1)}, bf16[4,16,4096]{2,1,0:T(8,128)(2,1)}, u32[]{:S(2)}) copy-start(bf16[4,16,4096]{2,1,0:T(8,128)(2,1)} %copy-done.2) | copy-start | bytes 1572868
  169.6 23.0 %copy-start.19 = (bf16[2,4096,256]{2,1,0:T(8,128)(2,1)S(1)}, bf16[2,4096,256]{2,1,0:T(8,128)(2,1)}, u32[]{:S(2)}) copy-start(bf16[2,4096,256]{2,1,0:T(8,128)(2,1)} %param.33) | copy-start | bytes 12582916
  189.3 3.2 %copy-start.13 = (bf16[64,16,4096]{2,1,0:T(8,128)(2,1)}, bf16[64,16,4096]{2,1,0:T(8,128)(2,1)S(1)}, u32[]{:S(2)}) copy-start(bf16[64,16,4096]{2,1,0:T(8,128)(2,1)S(1)} %constant_dynamic-update-slice_fusion) | copy-start | bytes 25165828
  202.9 55.4 %copy-start.17 = (f32[16,2]{0,1:T(2,128)S(1)}, f32[16,2]{0,1:T(2,128)}, u32[]{:S(2)}) copy-start(f32[16,2]{0,1:T(2,128)} %param.32) | copy-start | bytes 388
  202.9 63.4 %copy-start.11 = (bf16[16,4096]{1,0:T(8,128)(2,1)S(1)}, bf16[16,4096]{1,0:T(8,128)(2,1)}, u32[]{:S(2)}) copy-start(bf16[16,4096]{1,0:T(8,128)(2,1)} %reduce-scatter.3.cloned.1.call-done) | copy-start | bytes 393220
  254.3 10.2 %all-to-all-start.1 = ((bf16[4,16,4096]{2,1,0:T(8,128)(2,1)}), bf16[4,16,4096]{2,1,0:T(8,128)(2,1)S(1)}, u32[]{:S(2)}, u32[]{:S(2)}) async-start(bf16[4,16,4096]{2,1,0:T(8,128)(2,1)} %reduce-scatter.5.cloned.1.call-done), calls=%async_computation.3 | async-start | bytes 1048576 | tf_op jit(solution)/shard_map/all_to_all | solution.py:160
Sparse Core Ops, SparseCore 0:
  58.0 32.8 reduce-scatter.2
  207.7 46.5 reduce-scatter.4
